TPU v7x, 512 devices: a 4x2x32 block of a 4x8x32 slice. The times are simulated.
512 devices in a mesh: grp: 2 (over y), fs: 32 (over z), tp: 8 (over x, core).
Axes of the slice: x: 4, y: 2, z: 32, core: 2. Of those that a mesh axis runs over, the one named last changes fastest.
The devices are a block of a 4x8x32 slice.
Arguments:
- tokens: bfloat16 [12288, 2048], P(('grp', 'fs'), 'tp'), parts along dimension 0, may hold values from -40 to 40
- routes: int32 [12288, 8], P(('grp', 'fs')), parts along dimension 0, may hold values from 0 to 31, all different within a row; in each aligned block of 192 rows (0 to 191, 192 to 383, ...) at most 56 rows name the same one
- routing_weight: float32 [12288, 8], P(('grp', 'fs')), parts along dimension 0, may hold values from 0.1 to 0.6
- norm_gain_vector: float32 [2048], P('tp'), may hold values from 0.1 to 1.9
- expert_gate: float32 [32, 512, 2048], P(None, 'fs', 'tp'), may hold values from -0.125 to 0.125
- expert_up: float32 [32, 512, 2048], P(None, 'fs', 'tp'), may hold values from -0.125 to 0.125
- expert_down: float32 [32, 512, 2048], P(None, 'fs', 'tp'), may hold values from -0.25 to 0.25
- shared_gate: float32 [512, 2048], P('fs', 'tp'), may hold values from -0.125 to 0.125
- shared_up: float32 [512, 2048], P('fs', 'tp'), may hold values from -0.125 to 0.125
- shared_down: float32 [512, 2048], P('fs', 'tp'), may hold values from -0.25 to 0.25
Outputs:
- mixed: bfloat16 [12288, 2048], P(('grp', 'fs'), 'tp'), parts along dimension 0
- gate_served: bfloat16 [64, 512, 2048], P(('grp', 'fs'), None, 'tp'), parts along dimension 0
- up_served: bfloat16 [64, 512, 2048], P(('grp', 'fs'), None, 'tp'), parts along dimension 0
- down_served: bfloat16 [64, 512, 2048], P(('grp', 'fs'), None, 'tp'), parts along dimension 0
- shared_gate_served: bfloat16 [1024, 2048], P('grp', 'tp'), parts along dimension 0
- shared_up_served: bfloat16 [1024, 2048], P('grp', 'tp'), parts along dimension 0
- shared_down_served: bfloat16 [1024, 2048], P('grp', 'tp'), parts along dimension 0
There are 2 independent parts, one for each index of `grp`. A program takes and returns all parts, laid end to end along the dimension named above; an argument that names none is the same for every part. Nothing has to cross between parts.
Inputs may be any that keep to these rules, and one draw needn't show every extreme that they name: `routes`: each row names 8 different experts. In each aligned block of 192 rows no expert is named by more than 56 rows, and in some block an expert is named by exactly 56 rows.
All inputs are finite; a program needn't handle non-finite values.
Results may differ from a plain program's by a relative error of at most 0.022.
Values may be sent and summed in bfloat16 or wider, within the bound.
No kernel may reach another device: no remote copies, remote signals or barrier semaphores. Data moves between devices by JAX's collectives and lax.ppermute only.
A program may use at most 64 MiB of HBM per device.

v0:
```python
import jax
import jax.numpy as jnp
from jax import lax
from jax.sharding import PartitionSpec as P

norm_eps = 1e-06


def sent_together(arrays, axis, split_dim, concat_dim, along):
    widths = [a.shape[along] for a in arrays]
    both = jnp.concatenate(arrays, axis=along)
    out = lax.all_to_all(both, axis, split_axis=split_dim, concat_axis=concat_dim, tiled=True)
    return tuple(jnp.split(out, [sum(widths[:k]) for k in range(1, len(widths))], axis=along))


def sent_together_2(arrays, axis, dim, along):
    both = jnp.concatenate(arrays, axis=along)
    out, at, outs = (lax.all_gather(both, axis, axis=dim, tiled=True), 0, [])
    for a in arrays:
        outs.append(lax.slice_in_dim(out, at, at + a.shape[along], axis=along))
        at += a.shape[along]
    return tuple(outs)


def in_one_piece(arrays, axis, dim, along):
    both = jnp.concatenate(arrays, axis=along)
    out, at, outs = (lax.psum_scatter(both, axis, scatter_dimension=dim, tiled=True), 0, [])
    for a in arrays:
        outs.append(lax.slice_in_dim(out, at, at + a.shape[along], axis=along))
        at += a.shape[along]
    return tuple(outs)


def dense_rows(rows, weight):
    return lax.dot_general(
        rows, weight, (((1,), (1,)), ((), ())), preferred_element_type=jnp.float32
    )


def per_device(
    tokens,
    routes,
    routing_weight,
    norm_gain_vector,
    expert_gate,
    expert_up,
    expert_down,
    shared_gate,
    shared_up,
    shared_down,
):
    tok_rows, portion_width = tokens.shape
    model_width = portion_width * lax.axis_size("tp")
    experts = expert_gate.shape[0]
    top_count = routes.shape[1]
    capacity = tok_rows * top_count * 7 // (6 * experts)
    gate_round = (expert_gate * norm_gain_vector[None, None, :]).astype(jnp.bfloat16)
    up_round = (expert_up * norm_gain_vector[None, None, :]).astype(jnp.bfloat16)
    down_round = expert_down.astype(jnp.bfloat16)
    gate_refreshed, up_new, down_new = sent_together(
        (gate_round, up_round, down_round), "fs", 0, 1, 2
    )
    shared_g, shared_u, shared_d = sent_together_2(
        (
            (shared_gate * norm_gain_vector[None, :]).astype(jnp.bfloat16),
            (shared_up * norm_gain_vector[None, :]).astype(jnp.bfloat16),
            shared_down.astype(jnp.bfloat16),
        ),
        "fs",
        0,
        1,
    )
    values = tokens.astype(jnp.float32)
    totals = lax.psum(jnp.sum(values * values, axis=1), "tp")
    normed = (values * lax.rsqrt(totals / model_width + norm_eps)[:, None]).astype(jnp.bfloat16)
    flat_expert = routes.reshape(-1)
    onehot = (flat_expert[:, None] == jnp.arange(experts, dtype=jnp.int32)[None, :]).astype(
        jnp.int32
    )
    earlier = jnp.cumsum(onehot, axis=0) - onehot
    slot_index = jnp.sum(earlier * onehot, axis=1)
    target = (flat_expert * capacity + slot_index).reshape(tok_rows, top_count)
    places = jnp.arange(experts * capacity, dtype=jnp.int32)
    placing = jnp.sum(
        (target[:, :, None] == places[None, None, :]).astype(jnp.int32), axis=1
    ).astype(jnp.bfloat16)
    outgoing = lax.dot_general(
        placing, normed, (((0,), (0,)), ((), ())), preferred_element_type=jnp.float32
    ).astype(jnp.bfloat16)
    incoming = lax.all_to_all(
        outgoing.reshape(experts, capacity, portion_width),
        "fs",
        split_axis=0,
        concat_axis=0,
        tiled=True,
    )
    arrived = incoming.reshape(experts * capacity, portion_width)
    partials = (
        dense_rows(arrived, gate_refreshed[0]).astype(jnp.bfloat16),
        dense_rows(arrived, up_new[0]).astype(jnp.bfloat16),
        dense_rows(normed, shared_g).astype(jnp.bfloat16),
        dense_rows(normed, shared_u).astype(jnp.bfloat16),
    )
    gate_part, up_part, sgate_part, sup_part = tuple(
        (
            part.astype(jnp.float32)
            for part in in_one_piece(
                (partials[0], partials[1], partials[2], partials[3]), "tp", 1, 0
            )
        )
    )
    hidden, shared_hidden = (
        lax.all_gather(
            (jax.nn.silu(gate_part) * up_part).astype(jnp.bfloat16), "tp", axis=1, tiled=True
        ),
        lax.all_gather(
            (jax.nn.silu(sgate_part) * sup_part).astype(jnp.bfloat16), "tp", axis=1, tiled=True
        ),
    )
    produced = jnp.dot(hidden, down_new[0], preferred_element_type=jnp.float32).astype(jnp.bfloat16)
    returned = lax.all_to_all(
        produced.reshape(experts, capacity, portion_width),
        "fs",
        split_axis=0,
        concat_axis=0,
        tiled=True,
    )
    picked = returned.reshape(experts * capacity, portion_width)[target]
    routed = jnp.sum(routing_weight[:, :, None] * picked.astype(jnp.float32), axis=1)
    shared_out = jnp.dot(shared_hidden, shared_d, preferred_element_type=jnp.float32)
    mixed = (routed + shared_out).astype(jnp.bfloat16)
    return (mixed, gate_refreshed, up_new, down_new, shared_g, shared_u, shared_d)


def solution(mesh):
    return jax.shard_map(
        per_device,
        mesh=mesh,
        in_specs=(
            P(("grp", "fs"), "tp"),
            P(("grp", "fs"), None),
            P(("grp", "fs"), None),
            P("tp"),
            P(None, "fs", "tp"),
            P(None, "fs", "tp"),
            P(None, "fs", "tp"),
            P("fs", "tp"),
            P("fs", "tp"),
            P("fs", "tp"),
        ),
        out_specs=(
            P(("grp", "fs"), "tp"),
            P(("grp", "fs"), None, "tp"),
            P(("grp", "fs"), None, "tp"),
            P(("grp", "fs"), None, "tp"),
            P("grp", "tp"),
            P("grp", "tp"),
            P("grp", "tp"),
        ),
        check_vma=False,
    )
```

profile of v0, /device:TPU:33, one launch (start us, length us, event | category | flops | bytes accessed | tf_op | source)
XLA Modules:
  0.0 525.0 jit_solution(1667189688354686824)
XLA Ops:
  7.2 1.1 convert_element_type.88
  8.3 1.3 multiply_convert_fusion.1
  9.6 1.0 pad_maximum_fusion.1
  10.6 46.3 %all-to-all-start.1 = ((bf16[32,16,768]{2,1,0:T(8,128)(2,1)}), bf16[32,16,768]{2,1,0:T(8,128)(2,1)S(1)}, u32[]{:S(2)}, u32[]{:S(2)}) async-start(bf16[32,16,768]{2,1,0:T(8,128)(2,1)} %pad_maximum_fusion.1), calls=%async_computation.1 | async-start | bytes 1572864 | tf_op jit(solution)/shard_map/all_to_all | solution.py:12
  57.3 9.1 %reduce-window.6 = s32[32,12,128]{2,1,0:T(8,128)S(1)} reduce-window(s32[32,12,128]{2,1,0:T(8,128)S(1)} %fusion.11, s32[]{:T(128)} %constant.6.clone.1), window={size=1x1x128 pad=0_0x0_0x127_0}, to_apply=%region_0.0 | reduce-window | flops 6242304 | bytes 393220 | tf_op jit(solution)/shard_map/reduce-window
  67.5 13.3 %psum.7 = f32[192]{0:T(256)S(1)} all-reduce(f32[192]{0:T(256)S(1)} %fusion.12), channel_id=1, replica_groups=mesh['grp'=2,'fs'=32,'tp'=8] {'tp'}, use_global_device_ids=true, to_apply=%region_5.6 | all-reduce | flops 192 | bytes 1536 | tf_op jit(solution)/shard_map/psum | solution.py:74
  80.8 5.0 convert_reduce_fusion
  85.9 1.5 convolution_convert_fusion.3
  87.3 55.5 %all-to-all-done.1 = bf16[32,16,768]{2,1,0:T(8,128)(2,1)S(1)} async-done(((bf16[32,16,768]{2,1,0:T(8,128)(2,1)}), bf16[32,16,768]{2,1,0:T(8,128)(2,1)S(1)}, u32[]{:S(2)}, u32[]{:S(2)}) %all-to-all-start.1) | async-done | bytes 786464 | tf_op jit(solution)/shard_map/all_to_all | solution.py:12
  142.8 4.8 all-to-all-start
  147.8 122.6 %all_gather.9 = bf16[512,768]{1,0:T(8,128)(2,1)S(1)} all-gather(bf16[16,768]{1,0:T(8,128)(2,1)S(1)} %pad_maximum_fusion.2), channel_id=1, replica_groups=mesh['grp'=2,'fs'=32,'tp'=8] {'fs'}, dimensions={0}, use_global_device_ids=true | all-gather | bytes 811008 | tf_op jit(solution)/shard_map/all_gather | solution.py:18
  270.7 0.9 convolution_convert_fusion.5
  273.4 2.1 pad_maximum_fusion
  275.5 6.3 %copy.56 = bf16[3968,512]{0,1:T(8,128)(2,1)} copy(bf16[3968,512]{1,0:T(8,128)(2,1)} %pad_maximum_fusion) | data formatting | bytes 8126464
  282.1 64.3 %reduce-scatter.4.cloned.1.call-done = bf16[64,3968]{1,0:T(8,128)(2,1)} async-done(((bf16[512,3968]{1,0:T(8,128)(2,1)}), bf16[64,3968]{1,0:T(8,128)(2,1)}) %reduce-scatter.4.cloned.1.call-update) | async-done | bytes 507920
  346.4 1.9 fusion.7
  348.3 41.7 %all-gather.2.cloned.1.call-done = bf16[1792,512]{0,1:T(8,128)(2,1)} async-done(((bf16[1792,64]{0,1:T(8,128)(2,1)}), bf16[1792,512]{0,1:T(8,128)(2,1)}) %all-gather.2.cloned.1.call-update) | async-done | bytes 1835024 | tf_op jit(solution)/shard_map/all_gather | solution.py:113
  390.0 3.1 convolution_convert_fusion.2
  393.1 23.3 %all-to-all-start.2 = ((bf16[32,56,256]{2,1,0:T(8,128)(2,1)}), bf16[32,56,256]{2,1,0:T(8,128)(2,1)S(1)}, u32[]{:S(2)}, u32[]{:S(2)}) async-start(bf16[32,56,256]{2,1,0:T(8,128)(2,1)} %bitcast.8), calls=%async_computation.2 | async-start | bytes 1835008 | tf_op jit(solution)/shard_map/all_to_all | solution.py:121
  416.8 0.9 fusion.21
  417.7 13.4 %all_gather.11 = bf16[192,512]{0,1:T(8,128)(2,1)S(1)} all-gather(bf16[192,64]{0,1:T(8,128)(2,1)S(1)} %fusion.21), channel_id=1, replica_groups=mesh['grp'=2,'fs'=32,'tp'=8] {'tp'}, dimensions={1}, use_global_device_ids=true | all-gather | bytes 221184 | tf_op jit(solution)/shard_map/all_gather | solution.py:116
  431.2 80.7 %all-to-all-done.2 = bf16[32,56,256]{2,1,0:T(8,128)(2,1)S(1)} async-done(((bf16[32,56,256]{2,1,0:T(8,128)(2,1)}), bf16[32,56,256]{2,1,0:T(8,128)(2,1)S(1)}, u32[]{:S(2)}, u32[]{:S(2)}) %all-to-all-start.2) | async-done | bytes 917536 | tf_op jit(solution)/shard_map/all_to_all | solution.py:121
  511.9 4.8 gather_fusion
  517.2 0.9 fusion.1
  (62 shorter events, 4.7 us)
Async XLA Ops:
  9.6 47.3 %copy-start.8 = (s32[192,8]{0,1:T(8,128)S(1)}, s32[192,8]{0,1:T(8,128)}, u32[]{:S(2)}) copy-start(s32[192,8]{0,1:T(8,128)} %param.11) | copy-start | bytes 18436
  10.6 132.3 %all-to-all-start.1 = ((bf16[32,16,768]{2,1,0:T(8,128)(2,1)}), bf16[32,16,768]{2,1,0:T(8,128)(2,1)S(1)}, u32[]{:S(2)}, u32[]{:S(2)}) async-start(bf16[32,16,768]{2,1,0:T(8,128)(2,1)} %pad_maximum_fusion.1), calls=%async_computation.1 | async-start | bytes 1572864 | tf_op jit(solution)/shard_map/all_to_all | solution.py:12
  56.9 10.4 %copy-start = (bf16[192,256]{1,0:T(8,128)(2,1)S(1)}, bf16[192,256]{1,0:T(8,128)(2,1)}, u32[]{:S(2)}) copy-start(bf16[192,256]{1,0:T(8,128)(2,1)} %param.10) | copy-start | bytes 294916
  85.8 61.9 %copy-start.11 = (f32[16,256]{1,0:T(8,128)S(1)}, f32[16,256]{1,0:T(8,128)}, u32[]{:S(2)}) copy-start(f32[16,256]{1,0:T(8,128)} %param.19) | copy-start | bytes 49156
  85.8 62.0 %copy-start.9 = (f32[16,256]{1,0:T(8,128)S(1)}, f32[16,256]{1,0:T(8,128)}, u32[]{:S(2)}) copy-start(f32[16,256]{1,0:T(8,128)} %param.17) | copy-start | bytes 49156
  85.8 62.0 %copy-start.10 = (f32[16,256]{1,0:T(8,128)S(1)}, f32[16,256]{1,0:T(8,128)}, u32[]{:S(2)}) copy-start(f32[16,256]{1,0:T(8,128)} %param.18) | copy-start | bytes 49156
  85.9 62.0 %copy-start.13 = (f32[256]{0:T(256)S(1)}, f32[256]{0:T(256)}, u32[]{:S(2)}) copy-start(f32[256]{0:T(256)} %param.13) | copy-start | bytes 3076
  142.8 128.9 %all-to-all-start = ((bf16[32,56,256]{2,1,0:T(8,128)(2,1)}), bf16[32,56,256]{2,1,0:T(8,128)(2,1)S(1)}, u32[]{:S(2)}, u32[]{:S(2)}) async-start(bf16[32,56,256]{2,1,0:T(8,128)(2,1)} %bitcast.2), calls=%async_computation | async-start | bytes 1835008 | tf_op jit(solution)/shard_map/all_to_all | solution.py:90
  147.7 198.7 %reduce-scatter.4.cloned.1.call-start = ((), (), s32[]{:S(2)}) async-start(), calls=%async_computation.5 | async-start | bytes 4571136
  270.5 2.0 copy-start.4
  270.5 2.0 copy-start.5
  270.5 246.7 %copy-start.1 = (bf16[512,256]{1,0:T(8,128)(2,1)}, bf16[512,256]{1,0:T(8,128)(2,1)S(1)}, u32[]{:S(2)}) copy-start(bf16[512,256]{1,0:T(8,128)(2,1)S(1)} %get-tuple-element.9) | copy-start | bytes 786436
  271.7 1.4 copy-start.2
  271.7 1.4 copy-start.3
  271.8 118.2 %copy-start.7 = (bf16[1,512,256]{2,1,0:T(8,128)(2,1)}, bf16[1,512,256]{2,1,0:T(8,128)(2,1)S(1)}, u32[]{:S(2)}) copy-start(bf16[1,512,256]{2,1,0:T(8,128)(2,1)S(1)} %get-tuple-element.12) | copy-start | bytes 786436
  272.5 0.9 copy-start.6
  281.8 108.2 %all-gather.2.cloned.1.call-start = ((), (), s32[]{:S(2)}) async-start(), calls=%async_computation.4 | async-start | bytes 2064384 | tf_op jit(solution)/shard_map/all_gather | solution.py:113
  393.1 23.6 %copy-start.12 = (f32[192,8]{0,1:T(8,128)S(1)}, f32[192,8]{0,1:T(8,128)}, u32[]{:S(2)}) copy-start(f32[192,8]{0,1:T(8,128)} %param.12) | copy-start | bytes 18436
  393.1 118.8 %all-to-all-start.2 = ((bf16[32,56,256]{2,1,0:T(8,128)(2,1)}), bf16[32,56,256]{2,1,0:T(8,128)(2,1)S(1)}, u32[]{:S(2)}, u32[]{:S(2)}) async-start(bf16[32,56,256]{2,1,0:T(8,128)(2,1)} %bitcast.8), calls=%async_computation.2 | async-start | bytes 1835008 | tf_op jit(solution)/shard_map/all_to_all | solution.py:121
Sparse Core Ops, SparseCore 0:
  281.9 64.3 reduce-scatter.3
  348.5 41.4 all-gather.1
where the time goes:
time: 526 us; the launch traced here: 525 us
  waiting for transfers between devices  242 us (46%)
  blocking collectives  149 us (28%)
  starting transfers between devices  74.8 us (14%)
  other arithmetic  23.3 us (4%)
  between operations  14.5 us (3%)
  local copies, waits for them, and re-layouts  12.8 us (2%)
  matrix products  8.01 us (2%)
    all_gather x1, blocking collectives, sent_together_2(): out, at, outs = (lax.all_gather(both, axis, axis=dim, tiled=True), 0, [])  123 us
    all_to_all x1, waiting for transfers between devices, per_device(): lax.all_to_all(produced.reshape(experts, capacity, portion_width), 'fs',...  80.7 us
    unnamed x3, waiting for transfers between devices  64.4 us
    all_to_all x1, waiting for transfers between devices, sent_together(): lax.all_to_all(both, axis, split_axis=split_dim, concat_axis=concat_dim,...  55.5 us
    all_to_all x1, starting transfers between devices, sent_together(): lax.all_to_all(both, axis, split_axis=split_dim, concat_axis=concat_dim,...  46.3 us
    all_gather x1, waiting for transfers between devices, per_device(): lax.all_gather((jax.nn.silu(gate_part) * up_part).astype(jnp.bfloat16), '...  41.7 us
    all_to_all x1, starting transfers between devices, per_device(): lax.all_to_all(produced.reshape(experts, capacity, portion_width), 'fs',...  23.3 us
    all_gather x1, blocking collectives, per_device(): lax.all_gather((jax.nn.silu(sgate_part) * sup_part).astype(jnp.bfloat16),...  13.4 us
  transfers between devices with their start and end apart: 5, of which 4 were waited for; matrix products, arithmetic and copies ran while one was open for 4% of the time, Pallas kernels for 0%

commit v1 on v0

--- a/solution.py
+++ b/solution.py
@@ -2,6 +2,7 @@
 import jax.numpy as jnp
 from jax import lax
 from jax.sharding import PartitionSpec as P
+from jax.lax import all_to_all, axis_size
 
 norm_eps = 1e-06
 
@@ -109,10 +110,11 @@
             )
         )
     )
+    answer_the_keys = lambda x_local, axis_no: jnp.concatenate(
+        all_to_all(jnp.stack(axis_size("tp") * [x_local], axis=0), "tp", 0, 0), axis=axis_no
+    )
     hidden, shared_hidden = (
-        lax.all_gather(
-            (jax.nn.silu(gate_part) * up_part).astype(jnp.bfloat16), "tp", axis=1, tiled=True
-        ),
+        answer_the_keys((jax.nn.silu(gate_part) * up_part).astype(jnp.bfloat16), 1),
         lax.all_gather(
             (jax.nn.silu(sgate_part) * sup_part).astype(jnp.bfloat16), "tp", axis=1, tiled=True
         ),

time: 526 us -> 509 us (0.968)
  waiting for transfers between devices: 242 us -> 200 us
  blocking collectives: 149 us -> 179 us
    all_gather x1 -> x0, waiting for transfers between devices: 41.7 us -> none  [per_device(): lax.all_gather((jax.nn.silu(gate_part) * up_part).astype(jnp.bfloat16), '...]
    all_to_all x0 -> x1, blocking collectives: none -> 28.6 us  [per_device(): all_to_all(jnp.stack(axis_size('tp') * [x_local], axis=0), 'tp', 0, 0)]
    unnamed x3 -> x2, waiting for transfers between devices: 64.4 us -> 64.6 us
  transfers between devices with their start and end apart: 5 -> 4, of which waited for: 4 -> 3; matrix products, arithmetic and copies ran while one was open for 4% -> 4% of each run, Pallas kernels for 0% -> 0%
where the time goes in v1:
time: 509 us; the launch traced here: 508 us
  waiting for transfers between devices  200 us (39%)
  blocking collectives  179 us (35%)
  starting transfers between devices  73.3 us (14%)
  other arithmetic  22.6 us (4%)
  between operations  14.5 us (3%)
  local copies, waits for them, and re-layouts  12.9 us (3%)
  matrix products  6.46 us (1%)
    all_gather x1, blocking collectives, sent_together_2(): out, at, outs = (lax.all_gather(both, axis, axis=dim, tiled=True), 0, [])  123 us
    all_to_all x1, waiting for transfers between devices, per_device(): lax.all_to_all(produced.reshape(experts, capacity, portion_width), 'fs',...  79.5 us
    unnamed x2, waiting for transfers between devices  64.6 us
    all_to_all x1, waiting for transfers between devices, sent_together(): lax.all_to_all(both, axis, split_axis=split_dim, concat_axis=concat_dim,...  55.5 us
    all_to_all x1, starting transfers between devices, sent_together(): lax.all_to_all(both, axis, split_axis=split_dim, concat_axis=concat_dim,...  46.3 us
    all_to_all x1, blocking collectives, per_device(): all_to_all(jnp.stack(axis_size('tp') * [x_local], axis=0), 'tp', 0, 0)  28.6 us
    all_to_all x1, starting transfers between devices, per_device(): lax.all_to_all(produced.reshape(experts, capacity, portion_width), 'fs',...  22.1 us
    all_gather x1, blocking collectives, per_device(): lax.all_gather((jax.nn.silu(sgate_part) * sup_part).astype(jnp.bfloat16),...  14.2 us
  transfers between devices with their start and end apart: 4, of which 3 were waited for; matrix products, arithmetic and copies ran while one was open for 4% of the time, Pallas kernels for 0%

profile of v1, /device:TPU:33, one launch (start us, length us, event | category | flops | bytes accessed | tf_op | source)
XLA Modules:
  0.0 508.0 jit_solution(9677543404593068625)
XLA Ops:
  7.2 1.1 convert_element_type.88
  8.3 1.3 multiply_convert_fusion.1
  9.6 1.0 pad_maximum_fusion.1
  10.6 46.3 %all-to-all-start.1 = ((bf16[32,16,768]{2,1,0:T(8,128)(2,1)}), bf16[32,16,768]{2,1,0:T(8,128)(2,1)S(1)}, u32[]{:S(2)}, u32[]{:S(2)}) async-start(bf16[32,16,768]{2,1,0:T(8,128)(2,1)} %pad_maximum_fusion.1), calls=%async_computation.1 | async-start | bytes 1572864 | tf_op jit(solution)/shard_map/all_to_all | solution.py:13
  57.3 9.1 %reduce-window.6 = s32[32,12,128]{2,1,0:T(8,128)S(1)} reduce-window(s32[32,12,128]{2,1,0:T(8,128)S(1)} %fusion.11, s32[]{:T(128)} %constant.6.clone.1), window={size=1x1x128 pad=0_0x0_0x127_0}, to_apply=%region_0.0 | reduce-window | flops 6242304 | bytes 393220 | tf_op jit(solution)/shard_map/reduce-window
  67.4 13.3 %psum.7 = f32[192]{0:T(256)S(1)} all-reduce(f32[192]{0:T(256)S(1)} %fusion.12), channel_id=1, replica_groups=mesh['grp'=2,'fs'=32,'tp'=8] {'tp'}, use_global_device_ids=true, to_apply=%region_5.6 | all-reduce | flops 192 | bytes 1536 | tf_op jit(solution)/shard_map/psum | solution.py:75
  80.8 5.1 convert_reduce_fusion
  85.9 1.4 convolution_convert_fusion.3
  87.3 55.5 %all-to-all-done.1 = bf16[32,16,768]{2,1,0:T(8,128)(2,1)S(1)} async-done(((bf16[32,16,768]{2,1,0:T(8,128)(2,1)}), bf16[32,16,768]{2,1,0:T(8,128)(2,1)S(1)}, u32[]{:S(2)}, u32[]{:S(2)}) %all-to-all-start.1) | async-done | bytes 786464 | tf_op jit(solution)/shard_map/all_to_all | solution.py:13
  142.8 4.8 all-to-all-start
  147.8 122.6 %all_gather.6 = bf16[512,768]{1,0:T(8,128)(2,1)S(1)} all-gather(bf16[16,768]{1,0:T(8,128)(2,1)S(1)} %pad_maximum_fusion.2), channel_id=1, replica_groups=mesh['grp'=2,'fs'=32,'tp'=8] {'fs'}, dimensions={0}, use_global_device_ids=true | all-gather | bytes 811008 | tf_op jit(solution)/shard_map/all_gather | solution.py:19
  270.7 0.9 convolution_convert_fusion.5
  273.4 2.1 pad_maximum_fusion
  275.4 6.3 %copy.57 = bf16[3968,512]{0,1:T(8,128)(2,1)} copy(bf16[3968,512]{1,0:T(8,128)(2,1)} %pad_maximum_fusion) | data formatting | bytes 8126464
  281.8 64.6 %reduce-scatter.4.cloned.1.call-done = bf16[64,3968]{1,0:T(8,128)(2,1)} async-done(((bf16[512,3968]{1,0:T(8,128)(2,1)}), bf16[64,3968]{1,0:T(8,128)(2,1)}) %reduce-scatter.4.cloned.1.call-update) | async-done | bytes 507920
  346.3 1.2 fusion.7
  347.7 28.6 %all_to_all.27 = bf16[8,1792,64]{1,2,0:T(8,128)(2,1)S(1)} all-to-all(bf16[8,1792,64]{1,2,0:T(8,128)(2,1)S(1)} %stack.2), channel_id=1, replica_groups=mesh['grp'=2,'fs'=32,'tp'=8] {'tp'}, dimensions={0} | all-to-all | bytes 3670016 | tf_op jit(solution)/shard_map/all_to_all | solution.py:114
  376.3 1.6 convolution_convert_fusion.2
  377.9 22.1 %all-to-all-start.3 = ((bf16[32,56,256]{2,1,0:T(8,128)(2,1)}), bf16[32,56,256]{2,1,0:T(8,128)(2,1)S(1)}, u32[]{:S(2)}, u32[]{:S(2)}) async-start(bf16[32,56,256]{2,1,0:T(8,128)(2,1)} %bitcast.10), calls=%async_computation.3 | async-start | bytes 1835008 | tf_op jit(solution)/shard_map/all_to_all | solution.py:123
  400.4 0.9 fusion.21
  401.3 14.2 %all_gather.7 = bf16[192,512]{0,1:T(8,128)(2,1)S(1)} all-gather(bf16[192,64]{0,1:T(8,128)(2,1)S(1)} %fusion.21), channel_id=1, replica_groups=mesh['grp'=2,'fs'=32,'tp'=8] {'tp'}, dimensions={1}, use_global_device_ids=true | all-gather | bytes 221184 | tf_op jit(solution)/shard_map/all_gather | solution.py:118
  415.5 79.5 %all-to-all-done.3 = bf16[32,56,256]{2,1,0:T(8,128)(2,1)S(1)} async-done(((bf16[32,56,256]{2,1,0:T(8,128)(2,1)}), bf16[32,56,256]{2,1,0:T(8,128)(2,1)S(1)}, u32[]{:S(2)}, u32[]{:S(2)}) %all-to-all-start.3) | async-done | bytes 917536 | tf_op jit(solution)/shard_map/all_to_all | solution.py:123
  495.0 4.8 gather_fusion
  500.3 0.9 fusion.1
  (61 shorter events, 4.5 us)
Async XLA Ops:
  9.6 47.3 %copy-start.8 = (s32[192,8]{0,1:T(8,128)S(1)}, s32[192,8]{0,1:T(8,128)}, u32[]{:S(2)}) copy-start(s32[192,8]{0,1:T(8,128)} %param.11) | copy-start | bytes 18436
  10.6 132.3 %all-to-all-start.1 = ((bf16[32,16,768]{2,1,0:T(8,128)(2,1)}), bf16[32,16,768]{2,1,0:T(8,128)(2,1)S(1)}, u32[]{:S(2)}, u32[]{:S(2)}) async-start(bf16[32,16,768]{2,1,0:T(8,128)(2,1)} %pad_maximum_fusion.1), calls=%async_computation.1 | async-start | bytes 1572864 | tf_op jit(solution)/shard_map/all_to_all | solution.py:13
  56.9 10.4 %copy-start = (bf16[192,256]{1,0:T(8,128)(2,1)S(1)}, bf16[192,256]{1,0:T(8,128)(2,1)}, u32[]{:S(2)}) copy-start(bf16[192,256]{1,0:T(8,128)(2,1)} %param.10) | copy-start | bytes 294916
  85.8 61.9 %copy-start.11 = (f32[16,256]{1,0:T(8,128)S(1)}, f32[16,256]{1,0:T(8,128)}, u32[]{:S(2)}) copy-start(f32[16,256]{1,0:T(8,128)} %param.19) | copy-start | bytes 49156
  85.9 61.9 %copy-start.9 = (f32[16,256]{1,0:T(8,128)S(1)}, f32[16,256]{1,0:T(8,128)}, u32[]{:S(2)}) copy-start(f32[16,256]{1,0:T(8,128)} %param.17) | copy-start | bytes 49156
  85.9 61.9 %copy-start.10 = (f32[16,256]{1,0:T(8,128)S(1)}, f32[16,256]{1,0:T(8,128)}, u32[]{:S(2)}) copy-start(f32[16,256]{1,0:T(8,128)} %param.18) | copy-start | bytes 49156
  85.9 61.9 %copy-start.13 = (f32[256]{0:T(256)S(1)}, f32[256]{0:T(256)}, u32[]{:S(2)}) copy-start(f32[256]{0:T(256)} %param.13) | copy-start | bytes 3076
  142.8 128.9 %all-to-all-start = ((bf16[32,56,256]{2,1,0:T(8,128)(2,1)}), bf16[32,56,256]{2,1,0:T(8,128)(2,1)S(1)}, u32[]{:S(2)}, u32[]{:S(2)}) async-start(bf16[32,56,256]{2,1,0:T(8,128)(2,1)} %bitcast.2), calls=%async_computation | async-start | bytes 1835008 | tf_op jit(solution)/shard_map/all_to_all | solution.py:91
  147.7 198.7 %reduce-scatter.4.cloned.1.call-start = ((), (), s32[]{:S(2)}) async-start(), calls=%async_computation.5 | async-start | bytes 4571136
  270.4 2.0 copy-start.4
  270.4 2.0 copy-start.5
  270.5 229.8 %copy-start.1 = (bf16[512,256]{1,0:T(8,128)(2,1)}, bf16[512,256]{1,0:T(8,128)(2,1)S(1)}, u32[]{:S(2)}) copy-start(bf16[512,256]{1,0:T(8,128)(2,1)S(1)} %get-tuple-element.9) | copy-start | bytes 786436
  271.7 1.4 copy-start.2
  271.7 1.4 copy-start.3
  271.7 104.5 %copy-start.7 = (bf16[1,512,256]{2,1,0:T(8,128)(2,1)}, bf16[1,512,256]{2,1,0:T(8,128)(2,1)S(1)}, u32[]{:S(2)}) copy-start(bf16[1,512,256]{2,1,0:T(8,128)(2,1)S(1)} %get-tuple-element.12) | copy-start | bytes 786436
  272.5 0.9 copy-start.6
  377.9 22.4 %copy-start.12 = (f32[192,8]{0,1:T(8,128)S(1)}, f32[192,8]{0,1:T(8,128)}, u32[]{:S(2)}) copy-start(f32[192,8]{0,1:T(8,128)} %param.12) | copy-start | bytes 18436
  377.9 117.1 %all-to-all-start.3 = ((bf16[32,56,256]{2,1,0:T(8,128)(2,1)}), bf16[32,56,256]{2,1,0:T(8,128)(2,1)S(1)}, u32[]{:S(2)}, u32[]{:S(2)}) async-start(bf16[32,56,256]{2,1,0:T(8,128)(2,1)} %bitcast.10), calls=%async_computation.3 | async-start | bytes 1835008 | tf_op jit(solution)/shard_map/all_to_all | solution.py:123
Sparse Core Ops, SparseCore 0:
  281.9 64.3 reduce-scatter.3
